TPU v7x, 512 devices: a whole 4x4x16 slice. The times are simulated.
512 devices in a mesh: fs: 32 (over z, core), tp: 16 (over y, x).
Axes of the slice: x: 4, y: 4, z: 16, core: 2. Of those that a mesh axis runs over, the one named last changes fastest.
Arguments:
- tokens: bfloat16 [8192, 2048], P('fs', 'tp'), may hold values from -6 to 6
- norm_gain: float32 [2048], P('tp'), may hold values from 0.1 to 1.9
- gate_master: float32 [16, 3584, 2048], P(None, 'fs', 'tp'), may hold values from -0.125 to 0.125
- up_master: float32 [16, 3584, 2048], P(None, 'fs', 'tp'), may hold values from -0.125 to 0.125
- down_master: float32 [16, 3584, 2048], P(None, 'fs', 'tp'), may hold values from -0.0625 to 0.0625
- routes: int32 [8192, 2], P('fs'), may hold values from 0 to 7, all different within a row; in each aligned block of 256 rows (0 to 255, 256 to 511, ...) at most 64 rows name the same one
- route_logits: float32 [8192, 2], P('fs'), may hold values from -8 to 8
Outputs:
- gate_serve: bfloat16 [16, 3584, 2048], P('tp', 'fs')
- up_serve: bfloat16 [16, 3584, 2048], P('tp', 'fs')
- down_serve: bfloat16 [16, 3584, 2048], P('tp', 'fs')
- mixed_tokens: bfloat16 [8192, 2048], P('fs', 'tp')
Inputs may be any that keep to these rules, and one draw needn't show every extreme that they name: `routes`: each row names 2 different experts; in every aligned block of 256 rows each expert is named by exactly 64 rows.
All inputs are finite; a program needn't handle non-finite values.
Results may differ from a plain program's by a relative error of at most 0.024.
Values may be sent and summed in bfloat16 or wider, within the bound.
A program may use at most 64 MiB of HBM per device.

v0:
```python
import jax
import jax.numpy as jnp
from jax import lax
from jax.sharding import Mesh
from jax.sharding import PartitionSpec as P

FS = ("fs_0", "fs_1")


epsilon = 1e-05


def from_everyone(array, axis):
    copies = jnp.broadcast_to(array, (lax.axis_size(axis), *array.shape))
    return lax.all_to_all(copies, axis, split_axis=0, concat_axis=0, tiled=True)


def joined_along(parts, dim):
    parts = jnp.moveaxis(parts, 0, dim)
    lengths = parts.shape
    return parts.reshape(*lengths[:dim], lengths[dim] * lengths[dim + 1], *lengths[dim + 2 :])


def gathered_copies(array, axis, dim):
    parts = from_everyone(array, axis)
    return joined_along(parts, dim)


def side_by_side(arrays, axis, split_dim, concat_dim, along):
    widths = [a.shape[along] for a in arrays]
    both = jnp.concatenate(arrays, axis=along)
    result = lax.all_to_all(both, axis, split_axis=split_dim, concat_axis=concat_dim, tiled=True)
    return tuple(jnp.split(result, [sum(widths[:k]) for k in range(1, len(widths))], axis=along))


def partner(value, axis, apart):
    mask = 2**apart
    pairs = [(source, source ^ mask) for source in range(lax.axis_size(axis))]
    return lax.ppermute(value, axis, pairs)


def own_block(parts, axes, sequence):
    inside = parts.shape[1:]
    parts = parts.reshape(*(lax.axis_size(a) for a in axes), *inside)
    parts = jnp.moveaxis(parts, sequence, range(len(axes))).reshape(-1, *inside)
    for k in sequence:
        parts = lax.psum_scatter(parts, axes[k], scatter_dimension=0, tiled=True)
    return parts[0]


def cut_along(array, dim, count):
    before, after = (array.shape[:dim], array.shape[dim + 1 :])
    return jnp.moveaxis(array.reshape(*before, count, -1, *after), dim, 0)


def scatter_axes(array, axes, sequence, dim):
    count = lax.axis_size(axes)
    return own_block(cut_along(array, dim, count), axes, sequence)


def normalize(row_block):
    widened = row_block.astype(jnp.float32)
    row_scale = lax.rsqrt(jnp.mean(widened * widened, axis=-1, keepdims=True) + epsilon)
    return (widened * row_scale).astype(jnp.bfloat16)


def slab_hidden(inputs, gate_slab, up_slab):
    contract_dims = (((1,), (1,)), ((), ()))
    gate_pre = lax.dot_general(inputs, gate_slab, contract_dims, preferred_element_type=jnp.float32)
    up_pre = lax.dot_general(inputs, up_slab, contract_dims, preferred_element_type=jnp.float32)
    return (jax.nn.silu(gate_pre) * up_pre).astype(jnp.bfloat16)


def in_order(parity, mine, theirs):
    first = jnp.where(parity == 0, mine, theirs)
    second = jnp.where(parity == 0, theirs, mine)
    return (first, second)


def local(tokens, norm_gain, gate_master, up_master, down_master, routes, route_logits):
    tok_rows = tokens.shape[0]
    block_rows = gate_master.shape[1]
    slab_count = lax.axis_size("tp")
    experts = slab_count // 2
    capacity = tok_rows * routes.shape[1] // experts
    half_cap = capacity // 2
    own_expert = lax.axis_index("tp") // 2
    parity = lax.axis_index("tp") % 2
    gain_row = norm_gain[None, None, :]
    gate_ready = (gate_master * gain_row).astype(jnp.bfloat16)
    up_ready = (up_master * gain_row).astype(jnp.bfloat16)
    down_ready = down_master.astype(jnp.bfloat16)
    first_prob = jax.nn.sigmoid(route_logits[:, 0] - route_logits[:, 1])
    choice_prob = jnp.stack([first_prob, 1.0 - first_prob], axis=1)
    expert_ids = jnp.arange(experts, dtype=jnp.int32)
    matches = (routes[:, :, None] == expert_ids[None, None, :]).astype(jnp.float32)
    chosen = jnp.sum(matches, axis=1)
    weight = jnp.sum(matches * choice_prob[:, :, None], axis=1)
    position = jnp.cumsum(chosen, axis=0) - 1.0
    slot_ids = jnp.arange(capacity, dtype=jnp.float32)
    placed = chosen.T[:, None, :] * (position.T[:, None, :] == slot_ids[None, :, None]).astype(
        jnp.float32
    )
    own_pick = lax.dynamic_index_in_dim(placed, own_expert, 0, keepdims=False).astype(jnp.bfloat16)
    combine = (placed * weight.T[:, None, :]).reshape(experts * capacity, tok_rows)
    whole_rows = gathered_copies(tokens, "tp", 1)
    normed = normalize(whole_rows)
    gate_serve, up_serve, down_serve = side_by_side(
        (gate_ready, up_ready, down_ready), "tp", 0, 2, 1
    )
    other_gate, other_up, other_down = partner((gate_serve, up_serve, down_serve), "tp", 0)
    gate_pair = jnp.concatenate(in_order(parity, gate_serve, other_gate), axis=0)
    up_pair = jnp.concatenate(in_order(parity, up_serve, other_up), axis=0)
    down_both = jnp.concatenate(in_order(parity, down_serve, other_down), axis=0)
    half_pick = lax.dynamic_slice_in_dim(own_pick, parity * half_cap, half_cap, 0)
    picked = jnp.dot(half_pick, normed, preferred_element_type=jnp.float32).astype(jnp.bfloat16)
    row_piece = lax.all_gather(picked, FS, axis=0, tiled=True)
    hidden = jnp.concatenate(
        [
            slab_hidden(row_piece, gate_pair[0], up_pair[0]),
            slab_hidden(row_piece, gate_pair[1], up_pair[1]),
        ],
        axis=1,
    )
    down_pair = down_both.reshape(2 * block_rows, down_both.shape[2])
    row_piece = hidden
    expert_out = (
        scatter_axes(
            jnp.dot(row_piece, down_pair, preferred_element_type=jnp.float32).astype(jnp.bfloat16),
            FS,
            (1, 0),
            0,
        )
        .astype(jnp.float32)
        .astype(jnp.bfloat16)
    )
    returned = lax.all_to_all(expert_out, "tp", split_axis=1, concat_axis=0, tiled=True)
    mixed_tokens = jnp.dot(combine.T, returned.astype(jnp.float32))
    return (gate_serve, up_serve, down_serve, mixed_tokens.astype(jnp.bfloat16))


def solution(mesh):
    torus = Mesh(mesh.devices.reshape(16, 2, mesh.shape["tp"]), ("fs_0", "fs_1", "tp"))
    placed = (
        P(FS, "tp"),
        P("tp"),
        P(None, FS, "tp"),
        P(None, FS, "tp"),
        P(None, FS, "tp"),
        P(FS, None),
        P(FS, None),
    )
    return jax.shard_map(
        local,
        mesh=torus,
        in_specs=placed,
        out_specs=(P("tp", FS, None), P("tp", FS, None), P("tp", FS, None), P(FS, "tp")),
        check_vma=False,
    )
```

profile of v0, /device:TPU:2, one launch (start us, length us, event | category | flops | bytes accessed | tf_op | source)
XLA Modules:
  0.0 242.2 jit_solution(17516702112302546692)
XLA Ops:
  7.2 0.9 copy.22
  8.1 1.1 broadcast_in_dim.2
  9.2 9.3 %all-to-all-start.1 = ((bf16[16,256,128]{1,2,0:T(8,128)(2,1)}), bf16[16,256,128]{1,2,0:T(8,128)(2,1)S(1)}, u32[]{:S(2)}, u32[]{:S(2)}) async-start(bf16[16,256,128]{1,2,0:T(8,128)(2,1)} %broadcast_in_dim.2), calls=%async_computation.1 | async-start | bytes 2097152 | tf_op jit(solution)/shard_map/all_to_all | solution.py:15
  18.7 0.6 reduce-window.6
  19.3 0.2 slice_reduce_fusion
  19.6 0.1 fusion.1
  19.7 13.2 %all-to-all-done.1 = bf16[16,256,128]{1,2,0:T(8,128)(2,1)S(1)} async-done(((bf16[16,256,128]{1,2,0:T(8,128)(2,1)}), bf16[16,256,128]{1,2,0:T(8,128)(2,1)S(1)}, u32[]{:S(2)}, u32[]{:S(2)}) %all-to-all-start.1) | async-done | bytes 1048608 | tf_op jit(solution)/shard_map/all_to_all | solution.py:15
  32.9 0.3 multiply_reduce_fusion
  33.2 0.2 fusion
  33.5 1.1 convolution_convert_fusion.1
  34.7 0.1 multiply_convert_fusion.1
  34.9 0.1 pad_maximum_fusion
  35.0 21.3 %all_to_all.42 = bf16[16,336,128]{2,1,0:T(8,128)(2,1)S(1)} all-to-all(bf16[16,336,128]{2,1,0:T(8,128)(2,1)S(1)} %pad_maximum_fusion), channel_id=1, replica_groups=mesh['fs_0'=16,'fs_1'=2,'tp'=16] {'tp'}, dimensions={0} | all-to-all | bytes 2752512 | tf_op jit(solution)/shard_map/all_to_all | solution.py:32
  56.2 0.2 copy_bitcast_fusion
  56.4 0.1 fusion.29
  56.6 3.4 %collective-permute-start.2 = (bf16[1,112,2048]{2,1,0:T(8,128)(2,1)S(1)}, bf16[1,112,2048]{2,1,0:T(8,128)(2,1)S(1)}, u32[]{:S(2)}, u32[]{:S(2)}) collective-permute-start(bf16[1,112,2048]{2,1,0:T(8,128)(2,1)S(1)} %get-tuple-element.8), channel_id=1, source_target_pairs={{0,1},{1,0},{2,3},{3,2},{4,5},{5,4},{6,7},{7,6},{8,9},{9,8},{10,11... | collective-permute-start | bytes 1376264 | tf_op jit(solution)/shard_map/ppermute | solution.py:39
  60.0 2.5 %collective-permute-start.1 = (bf16[1,112,2048]{2,1,0:T(8,128)(2,1)S(1)}, bf16[1,112,2048]{2,1,0:T(8,128)(2,1)S(1)}, u32[]{:S(2)}, u32[]{:S(2)}) collective-permute-start(bf16[1,112,2048]{2,1,0:T(8,128)(2,1)S(1)} %get-tuple-element.9), channel_id=1, source_target_pairs={{0,1},{1,0},{2,3},{3,2},{4,5},{5,4},{6,7},{7,6},{8,9},{9,8},{10,11... | collective-permute-start | bytes 1376264 | tf_op jit(solution)/shard_map/ppermute | solution.py:39
  62.5 3.4 %collective-permute-start = (bf16[1,112,2048]{2,1,0:T(8,128)(2,1)S(1)}, bf16[1,112,2048]{2,1,0:T(8,128)(2,1)S(1)}, u32[]{:S(2)}, u32[]{:S(2)}) collective-permute-start(bf16[1,112,2048]{2,1,0:T(8,128)(2,1)S(1)} %get-tuple-element.10), channel_id=1, source_target_pairs={{0,1},{1,0},{2,3},{3,2},{4,5},{5,4},{6,7},{7,6},{8,9},{9,8},{10,11... | collective-permute-start | bytes 1376264 | tf_op jit(solution)/shard_map/ppermute | solution.py:39
  65.8 6.0 %collective-permute-done.2 = bf16[1,112,2048]{2,1,0:T(8,128)(2,1)S(1)} collective-permute-done((bf16[1,112,2048]{2,1,0:T(8,128)(2,1)S(1)}, bf16[1,112,2048]{2,1,0:T(8,128)(2,1)S(1)}, u32[]{:S(2)}, u32[]{:S(2)}) %collective-permute-start.2) | collective-permute-done | bytes 458784 | tf_op jit(solution)/shard_map/ppermute | solution.py:39
  72.0 14.8 %collective-permute-done = bf16[1,112,2048]{2,1,0:T(8,128)(2,1)S(1)} collective-permute-done((bf16[1,112,2048]{2,1,0:T(8,128)(2,1)S(1)}, bf16[1,112,2048]{2,1,0:T(8,128)(2,1)S(1)}, u32[]{:S(2)}, u32[]{:S(2)}) %collective-permute-start) | collective-permute-done | bytes 458784 | tf_op jit(solution)/shard_map/ppermute | solution.py:39
  86.8 22.8 %all-gather.2.cloned.1.call-done = bf16[1024,2048]{1,0:T(8,128)(2,1)} async-done(((bf16[32,2048]{1,0:T(8,128)(2,1)}), bf16[1024,2048]{1,0:T(8,128)(2,1)}) %all-gather.2.cloned.1.call-update) | async-done | bytes 4194320 | tf_op jit(solution)/shard_map/all_gather | solution.py:117
  109.6 3.8 %fusion.7 = f32[1024,112]{0,1:T(8,128)S(1)} fusion(bf16[1024,2048]{1,0:T(8,128)(2,1)} %all-gather.2.cloned.1.call-done, bf16[1,112,2048]{2,1,0:T(8,128)(2,1)S(1)} %collective-permute-done, bf16[1,112,2048]{2,1,0:T(8,128)(2,1)S(1)} %get-tuple-element.10, pred[]{:T(512)S(6)} %eq.50), kind=kOutput, calls=%fused_computation.18 | convolution fusion | flops 469991424 | bytes 5570561 | tf_op jit(solution)/shard_map/dot_general | solution.py:69
  113.4 1.5 fusion.11
  115.0 1.5 multiply_convert_fusion.2
  116.5 1.5 multiply_convert_fusion.3
  118.1 1.3 convolution_convert_fusion
  119.4 2.3 copy.23
  121.7 20.0 %reduce-scatter.3.cloned.1.call-done = bf16[16,32,2048]{2,1,0:T(8,128)(2,1)} async-done(((bf16[32,32,2048]{2,1,0:T(8,128)(2,1)}), bf16[16,32,2048]{2,1,0:T(8,128)(2,1)}) %reduce-scatter.3.cloned.1.call-update) | async-done | bytes 2097168 | tf_op jit(solution)/shard_map/reduce_scatter | solution.py:47
  141.8 78.3 %reduce-scatter.5.cloned.1.call-done = bf16[1,32,2048]{2,1,0:T(8,128)(2,1)} async-done(((bf16[16,32,2048]{2,1,0:T(8,128)(2,1)}), bf16[1,32,2048]{2,1,0:T(8,128)(2,1)}) %reduce-scatter.5.cloned.1.call-update) | async-done | bytes 131088 | tf_op jit(solution)/shard_map/reduce_scatter | solution.py:47
  220.1 0.9 copy.26
  221.1 13.7 %all_to_all.43 = bf16[32,16,128]{2,0,1:T(8,128)(2,1)S(1)} all-to-all(bf16[32,16,128]{2,0,1:T(8,128)(2,1)S(1)} %copy.24), channel_id=1, replica_groups=mesh['fs_0'=16,'fs_1'=2,'tp'=16] {'tp'}, dimensions={1} | all-to-all | bytes 262144 | tf_op jit(solution)/shard_map/all_to_all | solution.py:137
  234.7 0.9 fusion.30
  (38 shorter events, 0.6 us)
Async XLA Ops:
  7.2 11.5 %copy-start.8 = (f32[256,2]{0,1:T(2,128)S(1)}, f32[256,2]{0,1:T(2,128)}, u32[]{:S(2)}) copy-start(f32[256,2]{0,1:T(2,128)} %param.13) | copy-start | bytes 6148
  7.2 11.5 %copy-start.7 = (s32[256,2]{0,1:T(2,128)S(1)}, s32[256,2]{0,1:T(2,128)}, u32[]{:S(2)}) copy-start(s32[256,2]{0,1:T(2,128)} %param.12) | copy-start | bytes 6148
  9.2 23.7 %all-to-all-start.1 = ((bf16[16,256,128]{1,2,0:T(8,128)(2,1)}), bf16[16,256,128]{1,2,0:T(8,128)(2,1)S(1)}, u32[]{:S(2)}, u32[]{:S(2)}) async-start(bf16[16,256,128]{1,2,0:T(8,128)(2,1)} %broadcast_in_dim.2), calls=%async_computation.1 | async-start | bytes 2097152 | tf_op jit(solution)/shard_map/all_to_all | solution.py:15
  18.5 16.1 %copy-start.3 = (f32[16,112,128]{2,1,0:T(8,128)S(1)}, f32[16,112,128]{2,1,0:T(8,128)}, u32[]{:S(2)}) copy-start(f32[16,112,128]{2,1,0:T(8,128)} %param.11) | copy-start | bytes 2752516
  18.5 91.0 %all-gather.2.cloned.1.call-start = ((), (), s32[]{:S(2)}) async-start(), calls=%async_computation.5 | async-start | bytes 4325376 | tf_op jit(solution)/shard_map/all_gather | solution.py:117
  19.7 15.0 %copy-start.4 = (f32[16,112,128]{2,1,0:T(8,128)S(1)}, f32[16,112,128]{2,1,0:T(8,128)}, u32[]{:S(2)}) copy-start(f32[16,112,128]{2,1,0:T(8,128)} %param.9) | copy-start | bytes 2752516
  19.7 15.0 %copy-start.9 = (f32[128]{0:T(128)S(1)}, f32[128]{0:T(128)}, u32[]{:S(2)}) copy-start(f32[128]{0:T(128)} %param.8) | copy-start | bytes 1540
  33.5 1.3 copy-start.5
  34.6 107.2 %reduce-scatter.3.cloned.1.call-start = ((), (), s32[]{:S(2)}) async-start(), calls=%async_computation.6 | async-start | bytes 6291456 | tf_op jit(solution)/shard_map/reduce_scatter | solution.py:47
  56.6 56.8 %copy-start.1 = (bf16[1,112,2048]{2,1,0:T(8,128)(2,1)}, bf16[1,112,2048]{2,1,0:T(8,128)(2,1)S(1)}, u32[]{:S(2)}) copy-start(bf16[1,112,2048]{2,1,0:T(8,128)(2,1)S(1)} %get-tuple-element.10) | copy-start | bytes 1376260
  56.6 56.8 %copy-start.2 = (bf16[1,112,2048]{2,1,0:T(8,128)(2,1)}, bf16[1,112,2048]{2,1,0:T(8,128)(2,1)S(1)}, u32[]{:S(2)}) copy-start(bf16[1,112,2048]{2,1,0:T(8,128)(2,1)S(1)} %get-tuple-element.8) | copy-start | bytes 1376260
  56.6 59.9 %copy-start.6 = (bf16[1,112,2048]{2,1,0:T(8,128)(2,1)}, bf16[1,112,2048]{2,1,0:T(8,128)(2,1)S(1)}, u32[]{:S(2)}) copy-start(bf16[1,112,2048]{2,1,0:T(8,128)(2,1)S(1)} %get-tuple-element.9) | copy-start | bytes 1376260
  56.6 15.3 %collective-permute-start.2 = (bf16[1,112,2048]{2,1,0:T(8,128)(2,1)S(1)}, bf16[1,112,2048]{2,1,0:T(8,128)(2,1)S(1)}, u32[]{:S(2)}, u32[]{:S(2)}) collective-permute-start(bf16[1,112,2048]{2,1,0:T(8,128)(2,1)S(1)} %get-tuple-element.8), channel_id=1, source_target_pairs={{0,1},{1,0},{2,3},{3,2},{4,5},{5,4},{6,7},{7,6},{8,9},{9,8},{10,11... | collective-permute-start | bytes 1376264 | tf_op jit(solution)/shard_map/ppermute | solution.py:39
  60.0 55.0 %collective-permute-start.1 = (bf16[1,112,2048]{2,1,0:T(8,128)(2,1)S(1)}, bf16[1,112,2048]{2,1,0:T(8,128)(2,1)S(1)}, u32[]{:S(2)}, u32[]{:S(2)}) collective-permute-start(bf16[1,112,2048]{2,1,0:T(8,128)(2,1)S(1)} %get-tuple-element.9), channel_id=1, source_target_pairs={{0,1},{1,0},{2,3},{3,2},{4,5},{5,4},{6,7},{7,6},{8,9},{9,8},{10,11... | collective-permute-start | bytes 1376264 | tf_op jit(solution)/shard_map/ppermute | solution.py:39
  62.5 24.4 %collective-permute-start = (bf16[1,112,2048]{2,1,0:T(8,128)(2,1)S(1)}, bf16[1,112,2048]{2,1,0:T(8,128)(2,1)S(1)}, u32[]{:S(2)}, u32[]{:S(2)}) collective-permute-start(bf16[1,112,2048]{2,1,0:T(8,128)(2,1)S(1)} %get-tuple-element.10), channel_id=1, source_target_pairs={{0,1},{1,0},{2,3},{3,2},{4,5},{5,4},{6,7},{7,6},{8,9},{9,8},{10,11... | collective-permute-start | bytes 1376264 | tf_op jit(solution)/shard_map/ppermute | solution.py:39
  109.6 3.8 %copy-start = (bf16[1024,2048]{1,0:T(8,128)(2,1)S(1)}, bf16[1024,2048]{1,0:T(8,128)(2,1)}, u32[]{:S(2)}) copy-start(bf16[1024,2048]{1,0:T(8,128)(2,1)} %all-gather.2.cloned.1.call-done) | copy-start | bytes 12582916
  121.7 98.4 %reduce-scatter.5.cloned.1.call-start = ((), (), s32[]{:S(2)}) async-start(), calls=%async_computation.7 | async-start | bytes 2228224 | tf_op jit(solution)/shard_map/reduce_scatter | solution.py:47
Sparse Core Ops, SparseCore 0:
  34.7 74.8 all-gather.1
  121.8 19.9 reduce-scatter.2
  144.6 75.4 reduce-scatter.4
where the time goes:
time: 243 us; the launch traced here: 242 us
  waiting for transfers between devices  155 us (64%)
  blocking collectives  34.9 us (14%)
  starting transfers between devices  18.7 us (8%)
  between operations  14.1 us (6%)
  matrix products  11.7 us (5%)
  local copies, waits for them, and re-layouts  5.76 us (2%)
    reduce_scatter x2, waiting for transfers between devices, own_block(): parts = lax.psum_scatter(parts, axes[k], scatter_dimension=0, tiled=True)  98.4 us
    all_gather x1, waiting for transfers between devices, local(): row_piece = lax.all_gather(picked, FS, axis=0, tiled=True)  22.8 us
    all_to_all x1, blocking collectives, side_by_side(): lax.all_to_all(both, axis, split_axis=split_dim, concat_axis=concat_dim,...  21.3 us
    ppermute x3, waiting for transfers between devices, partner(): return lax.ppermute(value, axis, pairs)  20.8 us
    all_to_all x1, blocking collectives, local(): lax.all_to_all(expert_out, 'tp', split_axis=1, concat_axis=0, tiled=True)  13.7 us
    all_to_all x1, waiting for transfers between devices, from_everyone(): return lax.all_to_all(copies, axis, split_axis=0, concat_axis=0, tiled=True)  13.2 us
    all_to_all x1, starting transfers between devices, from_everyone(): return lax.all_to_all(copies, axis, split_axis=0, concat_axis=0, tiled=True)  9.32 us
    ppermute x3, starting transfers between devices, partner(): return lax.ppermute(value, axis, pairs)  9.21 us
  transfers between devices with their start and end apart: 7, of which 6 were waited for; matrix products, arithmetic and copies ran while one was open for 3% of the time, Pallas kernels for 0%

commit v1 on v0

v1 whole, which is shorter than its diff:
```python
import functools

import jax
import jax.numpy as jnp
from jax import lax
from jax.experimental import pallas as pl
from jax.experimental.pallas import tpu as pltpu
from jax.sharding import PartitionSpec as P

EPS = 1e-05
NX = 4
NT = 16
LANES = 128
MESH = pl.DeviceIdType.MESH
GROUPS = ((0, 2), (2, 1))
NG = len(GROUPS)


def kernel(
    nz,
    picked,
    wsrc,
    gate_out,
    up_out,
    down_out,
    ret,
    rows,
    ybuf,
    wbuf,
    xn,
    hid,
    part,
    rs_in,
    rs_out,
    eo,
    tok_s,
    tok_r,
    ag_s,
    ag_r,
    y_s,
    y_r,
    x_s,
    x_r,
    d_s,
    d_r,
    rs_s,
    rs_r,
    fin_s,
    fin_r,
    out_s,
):
    rb = rows.shape[1]
    width = rows.shape[2]
    fb = wsrc.shape[1] // NT
    pair = 2 * fb
    half = nz // 2
    cw = width // 2
    fs = lax.axis_index("fs")
    tp = lax.axis_index("tp")
    z, core = fs // 2, lax.rem(fs, 2)
    y, x = tp // NX, lax.rem(tp, NX)
    px, h = x // 2, lax.rem(x, 2)
    mate = {"tp": tp + 1 - 2 * h}
    cross = {"tp": y * NX + (NX - 1) - x}
    other_core = {"fs": fs + 1 - 2 * core}
    z_up = {"fs": lax.rem(z + 1, nz) * 2 + core}
    z_down = {"fs": lax.rem(z + nz - 1, nz) * 2 + core}
    z_dev = (z_up, z_down)
    pending = []

    def send(src, dst, s, r, dev):
        c = pltpu.make_async_remote_copy(
            src_ref=src, dst_ref=dst, send_sem=s, recv_sem=r, device_id=dev, device_id_type=MESH
        )
        c.start()
        pending.append(c)
        return c

    barrier = pltpu.get_barrier_semaphore()
    for k in range(1, NT):
        pl.semaphore_signal(
            barrier, inc=1, device_id={"tp": lax.rem(tp + k, NT)}, device_id_type=MESH
        )
    for dev in (other_core, z_up, z_down):
        pl.semaphore_signal(barrier, inc=1, device_id=dev, device_id_type=MESH)
    pl.semaphore_wait(barrier, NT - 1 + 3)

    lanes = lambda t: pl.ds(pl.multiple_of(t * LANES, LANES), LANES)
    frow = lambda i, n: pl.ds(pl.multiple_of(i * fb, fb), n * fb)
    my_rows = frow(2 * core, 2)

    tok = [None]
    for k in range(1, NT):
        t = lax.rem(tp + k, NT)
        tok.append(
            send(picked.at[t], rows.at[z, :, lanes(tp)], tok_s.at[k], tok_r.at[k], {"tp": t})
        )
    y_c = []
    for k in range(1, NX):
        ty = lax.rem(y + k, NX)
        dev = {"tp": ty * NX + x}
        per = []
        for g, (a, n) in enumerate(GROUPS):
            mine = send(
                wsrc.at[pl.ds(a, n), frow(ty * NX + 2 * px, 2), :],
                wbuf.at[pl.ds(a, n), my_rows, lanes(tp)],
                y_s.at[k - 1, g, 0],
                y_r.at[k - 1, g, 0],
                dev,
            )
            theirs = send(
                wsrc.at[pl.ds(a, n), frow(ty * NX + 2 - 2 * px, 2), :],
                ybuf.at[k - 1, pl.ds(a, n)],
                y_s.at[k - 1, g, 1],
                y_r.at[k - 1, g, 1],
                dev,
            )
            per.append((mine, theirs))
        y_c.append(per)

    x_c = {}

    def x_send(q):
        col = lax.rem(y + NX - q, NX) * NX + x
        for g, (a, n) in enumerate(GROUPS):
            if q:
                y_c[q - 1][g][0].wait_recv()
                y_c[q - 1][g][1].wait_recv()
                own = wbuf.at[pl.ds(a, n), my_rows, lanes(col)]
                oth = ybuf.at[q - 1, pl.ds(a, n)]
            else:
                own = wsrc.at[pl.ds(a, n), frow(y * NX + 2 * px, 2), :]
                oth = wsrc.at[pl.ds(a, n), frow(y * NX + 2 - 2 * px, 2), :]
            dst = wbuf.at[pl.ds(a, n), my_rows, lanes(col)]
            x_c[q, g, 1] = send(oth, dst, x_s.at[q, g, 1], x_r.at[q, g, 1], cross)
            x_c[q, g, 0] = send(own, dst, x_s.at[q, g, 0], x_r.at[q, g, 0], mate)

    def x_forward(q):
        col = lax.rem(y + NX - q, NX) * NX + (NX - 1) - x
        for g, (a, n) in enumerate(GROUPS):
            x_c[q, g, 1].wait_recv()
            ref = wbuf.at[pl.ds(a, n), my_rows, lanes(col)]
            x_c[q, g, 2] = send(ref, ref, x_s.at[q, g, 2], x_r.at[q, g, 2], mate)

    d_c = {}

    def core_send(q):
        cols = pl.ds(
            pl.multiple_of(lax.rem(y + NX - q, NX) * NX * LANES, NX * LANES), NX * LANES
        )
        for g, (a, n) in enumerate(GROUPS):
            x_c[q, g, 0].wait_recv()
            x_c[q, g, 2].wait_recv()
            ref = wbuf.at[pl.ds(a, n), my_rows, cols]
            d_c[q, g] = send(ref, ref, d_s.at[q, g], d_r.at[q, g], other_core)

    x_send(0)
    rows[z, :, lanes(tp)] = picked[tp]
    for a in range(3):
        wbuf[a, my_rows, lanes(tp)] = wsrc[a, frow(y * NX + 2 * px, 2), :]

    ag_c = {}

    def ag_chunks(s, d):
        return (0, 1) if s < half - 1 else (d,)

    def ag_send(s, d, c):
        b = lax.rem(z + (nz - s if d == 0 else s), nz)
        ref = rows.at[b, :, pl.ds(c * cw, cw)]
        ag_c[s, d, c] = send(ref, ref, ag_s.at[d, s, c], ag_r.at[d, s, c], z_dev[d])

    def ag_step(s):
        for c in (0, 1):
            for d in (0, 1):
                if s and c in ag_chunks(s - 1, d):
                    ag_c[s - 1, d, c].wait_recv()
                if s < half and c in ag_chunks(s, d):
                    ag_send(s, d, c)

    for k in range(1, NT):
        tok[k].wait_recv()
    ag_step(0)
    x_forward(0)
    ag_step(1)
    x_send(1)
    ag_step(2)
    x_send(3)
    x_forward(1)
    core_send(0)
    ag_step(3)
    x_forward(3)
    ag_step(4)
    core_send(1)
    ag_step(5)
    x_send(2)
    ag_step(6)
    core_send(3)
    x_forward(2)
    for s in range(7, half + 1):
        ag_step(s)

    @pl.loop(0, nz)
    def _(b):
        wide = rows[b].astype(jnp.float32)
        scale = lax.rsqrt(jnp.mean(wide * wide, axis=-1, keepdims=True) + EPS)
        xn[pl.ds(pl.multiple_of(b * rb, rb), rb), :] = (wide * scale).astype(jnp.bfloat16)

    core_send(2)
    outs = []
    for a, out in enumerate((gate_out, up_out, down_out)):
        c = pltpu.make_async_copy(wbuf.at[a, frow(2 * core + h, 1), :], out, out_s.at[a])
        c.start()
        outs.append(c)
    for q in range(NX):
        for g in range(NG):
            d_c[q, g].wait_recv()

    nt = (((1,), (1,)), ((), ()))

    @pl.loop(0, 2)
    def _(c):
        f = pl.ds(pl.multiple_of(c * pair, pair), pair)
        gate = lax.dot_general(xn[...], wbuf[0, f, :], nt, preferred_element_type=jnp.float32)
        up = lax.dot_general(xn[...], wbuf[1, f, :], nt, preferred_element_type=jnp.float32)
        hid[c] = (jax.nn.silu(gate) * up).astype(jnp.bfloat16)

    @pl.loop(0, width // 512)
    def _(i):
        cols = pl.ds(pl.multiple_of(i * 512, 512), 512)
        part[:, cols] = jnp.dot(
            hid[0], wbuf[2, pl.ds(0, pair), cols], preferred_element_type=jnp.float32
        ) + jnp.dot(hid[1], wbuf[2, pl.ds(pair, pair), cols], preferred_element_type=jnp.float32)

    rs_c = {}

    def term(b, c):
        return part[pl.ds(pl.multiple_of(b * rb, rb), rb), pl.ds(c * cw, cw)]

    for s in range(half):
        for c in (0, 1):
            for d in (0, 1):
                if s == 0 and c != d:
                    continue
                b = lax.rem(z + (half - s if d == 0 else half + s), nz)
                acc = term(b, c)
                if (s - 1, d, c) in rs_c:
                    rs_c[s - 1, d, c].wait_recv()
                    acc = acc + rs_in[d, s - 1, c].astype(jnp.float32)
                rs_out[d, s, c] = acc.astype(jnp.bfloat16)
                rs_c[s, d, c] = send(
                    rs_out.at[d, s, c],
                    rs_in.at[d, s, c],
                    rs_s.at[d, s, c],
                    rs_r.at[d, s, c],
                    z_dev[d],
                )
    for c in (0, 1):
        acc = term(z, c)
        for d in (0, 1):
            rs_c[half - 1, d, c].wait_recv()
            acc = acc + rs_in[d, half - 1, c].astype(jnp.float32)
        eo[:, pl.ds(c * cw, cw)] = acc.astype(jnp.bfloat16)

    fin = []
    mine = pl.ds(pl.multiple_of(tp * rb, rb), rb)
    for k in range(1, NT):
        t = lax.rem(tp + k, NT)
        fin.append(
            send(eo.at[:, lanes(t)], ret.at[mine, :], fin_s.at[k], fin_r.at[k], {"tp": t})
        )
    ret[mine, :] = eo[:, lanes(tp)]
    for c in fin:
        c.wait_recv()
    for c in outs:
        c.wait()
    for c in pending:
        c.wait_send()


def exchange(picked, wsrc, nz):
    rb, width, fb = picked.shape[1], NT * LANES, wsrc.shape[1] // NT
    half, cw = nz // 2, width // 2
    bf16, f32 = jnp.bfloat16, jnp.float32
    dma = pltpu.SemaphoreType.DMA
    vmem = pl.BlockSpec(memory_space=pltpu.VMEM)
    hbm = pl.BlockSpec(memory_space=pl.ANY)
    return pl.pallas_call(
        functools.partial(kernel, nz),
        name="exchange",
        out_shape=[jax.ShapeDtypeStruct((1, fb, width)[1:], bf16)] * 3
        + [jax.ShapeDtypeStruct((NT * rb, LANES), bf16)],
        in_specs=[vmem, vmem],
        out_specs=[hbm, hbm, hbm, vmem],
        scratch_shapes=[
            pltpu.VMEM((nz, rb, width), bf16),
            pltpu.VMEM((NX - 1, 3, 2 * fb, LANES), bf16),
            pltpu.VMEM((3, 4 * fb, width), bf16),
            pltpu.VMEM((nz * rb, width), bf16),
            pltpu.VMEM((2, nz * rb, 2 * fb), bf16),
            pltpu.VMEM((nz * rb, width), f32),
            pltpu.VMEM((2, half, 2, rb, cw), bf16),
            pltpu.VMEM((2, half, 2, rb, cw), bf16),
            pltpu.VMEM((rb, width), bf16),
            dma((NT,)),
            dma((NT,)),
            dma((2, half, 2)),
            dma((2, half, 2)),
            dma((NX - 1, NG, 2)),
            dma((NX - 1, NG, 2)),
            dma((NX, NG, 3)),
            dma((NX, NG, 3)),
            dma((NX, NG)),
            dma((NX, NG)),
            dma((2, half, 2)),
            dma((2, half, 2)),
            dma((NT,)),
            dma((NT,)),
            dma((3,)),
        ],
        compiler_params=pltpu.CompilerParams(collective_id=0, has_side_effects=True),
    )(picked, wsrc)


def local(tokens, norm_gain, gate_master, up_master, down_master, routes, route_logits):
    tok_rows = tokens.shape[0]
    experts = NT // 2
    capacity = tok_rows * 2 // experts
    fb = gate_master.shape[1]
    gain_row = norm_gain[None, None, :]
    wsrc = jnp.stack(
        [
            (gate_master * gain_row).astype(jnp.bfloat16),
            (up_master * gain_row).astype(jnp.bfloat16),
            down_master.astype(jnp.bfloat16),
        ]
    ).reshape(3, NT * fb, LANES)
    first_prob = jax.nn.sigmoid(route_logits[:, 0] - route_logits[:, 1])
    ids = jnp.arange(experts, dtype=jnp.int32)
    match = [routes[:, k][:, None] == ids[None, :] for k in (0, 1)]
    chosen = (match[0] | match[1]).astype(jnp.bfloat16)
    row_ids = jnp.arange(tok_rows, dtype=jnp.int32)
    before = (row_ids[None, :] < row_ids[:, None]).astype(jnp.bfloat16)
    position = jnp.dot(before, chosen, preferred_element_type=jnp.float32).astype(jnp.int32)
    slot_of = ids[None, :] * capacity + position
    slots = jnp.arange(experts * capacity, dtype=jnp.int32)
    hot = []
    for k in (0, 1):
        slot = jnp.sum(jnp.where(match[k], slot_of, 0), axis=1)
        hot.append((slot[:, None] == slots[None, :]).astype(jnp.bfloat16))
    both = hot[0] + hot[1]
    picked = lax.dot_general(
        both, tokens, (((0,), (0,)), ((), ())), preferred_element_type=jnp.float32
    ).astype(jnp.bfloat16)
    nz = lax.axis_size("fs") // 2
    gate_serve, up_serve, down_serve, ret = exchange(
        picked.reshape(NT, capacity // 2, LANES), wsrc, nz
    )
    sent = [jnp.dot(m, ret, preferred_element_type=jnp.float32) for m in hot]
    mixed = first_prob[:, None] * sent[0] + (1.0 - first_prob)[:, None] * sent[1]
    return (gate_serve[None], up_serve[None], down_serve[None], mixed.astype(jnp.bfloat16))


def solution(mesh):
    weights = P(None, "fs", "tp")
    served = P("tp", "fs", None)
    return jax.shard_map(
        local,
        mesh=mesh,
        in_specs=(P("fs", "tp"), P("tp"), weights, weights, weights, P("fs"), P("fs")),
        out_specs=(served, served, served, P("fs", "tp")),
        check_vma=False,
    )
```

time: 243 us -> 115 us (0.47)
  the two profiles are of different devices: /device:TPU:2 before, /device:TPU:8 now
where the time goes in v1:
time: 115 us
  Pallas kernels  103 us (90%)
  matrix products  4.35 us (4%)
  local copies, waits for them, and re-layouts  4.18 us (4%)
  other arithmetic  3.02 us (3%)
    pallas_call x1, Pallas kernels, exchange(): pl.pallas_call(functools.partial(kernel, nz), name='exchange', out_shape=...  103 us
    unnamed x13, local copies, waits for them, and re-layouts  3.42 us
    dot_general x2, matrix products, local(): sent = [jnp.dot(m, ret, preferred_element_type=jnp.float32) for m in hot]  3.08 us

profile of v1, /device:TPU:8, one launch (start us, length us, event | category | flops | bytes accessed | tf_op | source)
XLA Modules:
  0.0 115.0 jit_solution(5177888246278072222)
XLA Ops:
  0.6 0.0 copy-start
  0.6 0.8 fusion.16
  1.4 0.2 select_reduce_fusion.1
  1.6 0.0 copy-done
  1.6 1.1 convolution_convert_fusion
  2.7 0.0 copy-start.1
  2.7 1.7 %multiply_convert_fusion.1 = (bf16[16,112,128]{2,1,0:T(8,128)(2,1)S(1)}, bf16[16,112,128]{2,1,0:T(8,128)(2,1)S(1)}) fusion(f32[16,112,128]{2,1,0:T(8,128)} %param.9, f32[128]{0:T(128)} %param.8, f32[16,112,128]{2,1,0:T(8,128)} %param.10), kind=kLoop, calls=%fused_computation.9 | loop fusion | flops 917504 | bytes 2753024 | tf_op jit(solution)/shard_map/convert_element_type | solution.py:332
  4.4 0.0 copy-done.1
  4.4 0.1 convert_element_type.32
  4.5 1.2 %pad_maximum_fusion.wsrc = bf16[3,1792,128]{2,1,0:T(8,128)(2,1)} fusion(bf16[1,1792,128]{2,1,0:T(8,128)(2,1)S(1)} %bitcast.16, bf16[1,1792,128]{2,1,0:T(8,128)(2,1)S(1)} %bitcast.15, bf16[1,1792,128]{2,1,0:T(8,128)(2,1)S(1)} %bitcast.14), kind=kLoop, calls=%fused_computation | loop fusion | flops 1376256 | bytes 2752512 | tf_op jit(solution)/shard_map/stack | solution.py:330
  5.8 0.0 copy-start.4
  5.8 102.7 %exchange.1 = (bf16[112,2048]{1,0:T(8,128)(2,1)}, bf16[112,2048]{1,0:T(8,128)(2,1)}, bf16[112,2048]{1,0:T(8,128)(2,1)}, bf16[512,128]{1,0:T(8,128)(2,1)}) custom-call(bf16[16,32,128]{2,1,0:T(8,128)(2,1)} %bitcast.20, bf16[3,1792,128]{2,1,0:T(8,128)(2,1)} %pad_maximum_fusion.wsrc), custom_call_target="tpu_custom_call" | custom-call | tf_op jit(solution)/shard_map/exchange/pallas_call | solution.py:287
  108.5 0.0 copy-start.3
  108.5 0.0 copy-start.2
  108.5 0.0 copy-done.4
  108.5 1.3 %convolution_multiply_fusion.1 = f32[256,128]{1,0:T(8,128)S(1)} fusion(bf16[512,128]{1,0:T(8,128)(2,1)} %get-tuple-element.11, s32[256]{0:T(256)S(1)} %get-tuple-element.12, f32[256]{0:T(256)S(1)} %bitcast.24), kind=kOutput, calls=%fused_computation.4 | convolution fusion | flops 33718272 | bytes 264192 | tf_op jit(solution)/shard_map/dot_general | solution.py:358
  109.8 1.8 %fusion.1 = bf16[256,128]{1,0:T(8,128)(2,1)} fusion(f32[256,128]{1,0:T(8,128)S(1)} %convolution_multiply_fusion.1, bf16[512,128]{1,0:T(8,128)(2,1)} %get-tuple-element.11, s32[256]{0:T(256)S(1)} %get-tuple-element.13, f32[256]{0:T(256)S(1)} %bitcast.21), kind=kOutput, calls=%fused_computation.5 | convolution fusion | flops 33783808 | bytes 329728 | tf_op jit(solution)/shard_map/dot_general | solution.py:358
  111.6 1.8 %copy.14 = bf16[1,112,2048]{2,1,0:T(8,128)(2,1)} copy(bf16[1,112,2048]{2,1,0:T(8,128)(2,1)} %bitcast.19) | data formatting | bytes 917504
  113.4 0.0 copy-done.3
  113.4 0.8 copy.15
  114.2 0.0 copy-done.2
  114.2 0.8 copy.16
  (2 shorter events, 0.0 us)
Async XLA Ops:
  0.6 1.0 copy-start
  2.7 1.7 %copy-start.1 = (f32[16,112,128]{2,1,0:T(8,128)S(1)}, f32[16,112,128]{2,1,0:T(8,128)}, u32[]{:S(2)}) copy-start(f32[16,112,128]{2,1,0:T(8,128)} %param.11) | copy-start | bytes 2752516
  5.8 102.7 %copy-start.4 = (f32[256,2]{0,1:T(2,128)S(1)}, f32[256,2]{0,1:T(2,128)}, u32[]{:S(2)}) copy-start(f32[256,2]{0,1:T(2,128)} %param.13) | copy-start | bytes 6148
  108.5 4.9 %copy-start.3 = (bf16[112,2048]{1,0:T(8,128)(2,1)S(1)}, bf16[112,2048]{1,0:T(8,128)(2,1)}, u32[]{:S(2)}) copy-start(bf16[112,2048]{1,0:T(8,128)(2,1)} %get-tuple-element.9) | copy-start | bytes 1376260
  108.5 5.7 %copy-start.2 = (bf16[112,2048]{1,0:T(8,128)(2,1)S(1)}, bf16[112,2048]{1,0:T(8,128)(2,1)}, u32[]{:S(2)}) copy-start(bf16[112,2048]{1,0:T(8,128)(2,1)} %get-tuple-element.10) | copy-start | bytes 1376260

commit v2 on v1

v2 whole, which is shorter than its diff:
```python
import contextlib
import functools

import jax
import jax.numpy as jnp
from jax import lax
from jax.experimental import pallas as pl
from jax.experimental.pallas import tpu as pltpu
from jax.sharding import PartitionSpec as P

EPS = 1e-05
NX = 4
NT = 16
LANES = 128
QC = NX * LANES
MESH = pl.DeviceIdType.MESH
GROUPS = ((0, 2), (2, 1))
NG = len(GROUPS)
QORD = (0, 1, 3, 2)
SPLIT = ((0, 1), (3, 2))
SCOPED = False
ORDER = (
    "T0 T1 T3 T2 F0a X0b A1 X1a X3a Ra A2 F1a F3a F0b A3 X2a C0a C1a A4 F2a C3a X1b X3b Rb A5 "
    "F1b F3b C0b X2b A6 C2a F2b C1b A7 C3b H A8 C2b"
).split()


def scope(name):
    return jax.named_scope(name) if SCOPED else contextlib.nullcontext()


def kernel(
    nz,
    tokens_h,
    gain_h,
    gate_h,
    up_h,
    down_h,
    routes_h,
    logits_h,
    gate_out,
    up_out,
    down_out,
    mixed_out,
    tokens,
    gain,
    masters,
    routes,
    logits,
    wsrc,
    picked,
    cols8,
    rows,
    scales,
    ybuf,
    relay,
    wbuf,
    hid,
    part,
    rs_in,
    rs_out,
    eo,
    ret,
    in_s,
    tok_s,
    tok_r,
    ag_s,
    ag_r,
    y_s,
    y_r,
    w_s,
    w_r,
    x_s,
    x_r,
    d_s,
    d_r,
    rs_s,
    rs_r,
    fin_s,
    fin_r,
    out_s,
):
    tr = tokens.shape[0]
    width = rows.shape[1]
    rb = rows.shape[0] // nz
    fb = wsrc.shape[1] // NT
    pair = 2 * fb
    half = nz // 2
    f32, bf16 = jnp.float32, jnp.bfloat16
    fs = lax.axis_index("fs")
    tp = lax.axis_index("tp")
    z, core = fs // 2, lax.rem(fs, 2)
    y, x = tp // NX, lax.rem(tp, NX)
    px, h = x // 2, lax.rem(x, 2)
    mate = {"tp": tp + 1 - 2 * h}
    cross = {"tp": y * NX + (NX - 1) - x}
    other_core = {"fs": fs + 1 - 2 * core}
    z_up = {"fs": lax.rem(z + 1, nz) * 2 + core}
    z_down = {"fs": lax.rem(z + nz - 1, nz) * 2 + core}
    z_dev = (z_up, z_down)
    pending = []

    def send(src, dst, s, r, dev):
        c = pltpu.make_async_remote_copy(
            src_ref=src, dst_ref=dst, send_sem=s, recv_sem=r, device_id=dev, device_id_type=MESH
        )
        c.start()
        pending.append(c)
        return c

    def plane(dy, dx):
        return lax.rem(y + dy, NX) * NX + lax.rem(x + dx, NX)

    barrier = pltpu.get_barrier_semaphore()
    for k in range(1, NT):
        pl.semaphore_signal(
            barrier, inc=1, device_id={"tp": lax.rem(tp + k, NT)}, device_id_type=MESH
        )
    for dev in (other_core, z_up, z_down):
        pl.semaphore_signal(barrier, inc=1, device_id=dev, device_id_type=MESH)

    loads = []
    for i, (src, dst) in enumerate(
        (
            (routes_h, routes),
            (logits_h, logits),
            (tokens_h, tokens),
            (gain_h, gain),
            (gate_h, masters.at[0]),
            (up_h, masters.at[1]),
            (down_h, masters.at[2]),
        )
    ):
        c = pltpu.make_async_copy(src, dst, in_s.at[i])
        c.start()
        loads.append(c)

    lanes = lambda t: pl.ds(pl.multiple_of(t * LANES, LANES), LANES)
    frow = lambda i, n: pl.ds(pl.multiple_of(i * fb, fb), n * fb)
    chunk = lambda q: pl.ds(pl.multiple_of(lax.rem(y + NX - q, NX) * QC, QC), QC)
    src_tp = lambda q, xx: lax.rem(y + NX - q, NX) * NX + xx
    my_rows = frow(2 * core, 2)

    with scope("prep"):
        for c in loads[:4]:
            c.wait()
        e = lax.broadcasted_iota(jnp.int32, (NT // 2, tr), 0)
        m0 = e == routes[0:1, :]
        m1 = e == routes[1:2, :]
        chosen = jnp.where(m0 | m1, 1.0, 0.0).astype(bf16)
        earlier = lax.broadcasted_iota(jnp.int32, (tr, tr), 0) < lax.broadcasted_iota(
            jnp.int32, (tr, tr), 1
        )
        pos = jnp.dot(
            chosen, jnp.where(earlier, 1.0, 0.0).astype(bf16), preferred_element_type=f32
        )
        slot = pos + (2 * rb) * e.astype(f32)
        s0 = jnp.sum(jnp.where(m0, slot, 0.0), axis=0, keepdims=True)
        s1 = jnp.sum(jnp.where(m1, slot, 0.0), axis=0, keepdims=True)
        ids = lax.broadcasted_iota(jnp.int32, (NT * rb, tr), 0).astype(f32)
        hot = jnp.where((ids == s0) | (ids == s1), 1.0, 0.0).astype(bf16)
        picked[...] = jnp.dot(hot, tokens[...], preferred_element_type=f32).astype(bf16)
        p0 = jax.nn.sigmoid(logits[0:1, :] - logits[1:2, :])
        table = jnp.concatenate([s0, s1, p0, 1.0 - p0, jnp.zeros((4, tr), f32)], axis=0)
        cols8[...] = table.T
        for a in range(3):
            loads[4 + a].wait()
            if a < 2:
                wsrc[a] = (masters[a] * gain[...]).astype(bf16)
            else:
                wsrc[a] = masters[a].astype(bf16)
    with scope("barrier"):
        pl.semaphore_wait(barrier, NT - 1 + 3)

    prow = lambda t: pl.ds(pl.multiple_of(t * rb, rb), rb)
    tok = {}
    for dy in QORD:
        for dx in range(NX):
            if dy or dx:
                t = plane(dy, dx)
                tok[dy, dx] = send(
                    picked.at[prow(t), :],
                    rows.at[pl.ds(0, rb), lanes(tp)],
                    tok_s.at[dy, dx],
                    tok_r.at[dy, dx],
                    {"tp": t},
                )

    y_c, w_c = {}, {}

    def y_send(g):
        a, n = GROUPS[g]
        ks = pl.ds(a, n)
        for k in (1, 3):
            ty = lax.rem(y + k, NX)
            dev = {"tp": ty * NX + x}
            y_c[k, g, 0] = send(
                wsrc.at[ks, frow(ty * NX + 2 * px, 2), :],
                wbuf.at[ks, my_rows, lanes(tp)],
                y_s.at[k - 1, g, 0],
                y_r.at[k - 1, g, 0],
                dev,
            )
            y_c[k, g, 1] = send(
                wsrc.at[ks, frow(ty * NX + 2 - 2 * px, 2), :],
                ybuf.at[k - 1, ks],
                y_s.at[k - 1, g, 1],
                y_r.at[k - 1, g, 1],
                dev,
            )
        ty = lax.rem(y + 2, NX)
        for i, (first, via) in enumerate(((2 * px, 1), (2 - 2 * px, 3))):
            w_c[g, i] = send(
                wsrc.at[ks, frow(ty * NX + first, 2), :],
                relay.at[i, ks],
                w_s.at[g, i],
                w_r.at[g, i],
                {"tp": lax.rem(y + via, NX) * NX + x},
            )

    def y_relay(g):
        a, n = GROUPS[g]
        ks = pl.ds(a, n)
        for i, via in enumerate((1, 3)):
            w_c[g, i].wait_recv()
            dst = wbuf.at[ks, my_rows, lanes(src_tp(via, x))] if i == 0 else ybuf.at[1, ks]
            y_c[2, g, i] = send(
                relay.at[i, ks],
                dst,
                y_s.at[1, g, i],
                y_r.at[1, g, i],
                {"tp": lax.rem(y + via, NX) * NX + x},
            )

    x_c = {}

    def x_send(q, g):
        a, n = GROUPS[g]
        ks = pl.ds(a, n)
        dst = wbuf.at[ks, my_rows, lanes(src_tp(q, x))]
        if q:
            y_c[q, g, 1].wait_recv()
            oth = ybuf.at[q - 1, ks]
        else:
            oth = wsrc.at[ks, frow(y * NX + 2 - 2 * px, 2), :]
        x_c[q, g, 1] = send(oth, dst, x_s.at[q, g, 1], x_r.at[q, g, 1], cross)
        if q:
            y_c[q, g, 0].wait_recv()
            own = dst
        else:
            own = wsrc.at[ks, frow(y * NX + 2 * px, 2), :]
        x_c[q, g, 0] = send(own, dst, x_s.at[q, g, 0], x_r.at[q, g, 0], mate)

    def x_forward(q, g):
        a, n = GROUPS[g]
        x_c[q, g, 1].wait_recv()
        ref = wbuf.at[pl.ds(a, n), my_rows, lanes(src_tp(q, (NX - 1) - x))]
        x_c[q, g, 2] = send(ref, ref, x_s.at[q, g, 2], x_r.at[q, g, 2], mate)

    d_c = {}

    def core_send(q, g):
        a, n = GROUPS[g]
        x_c[q, g, 0].wait_recv()
        x_c[q, g, 2].wait_recv()
        ref = wbuf.at[pl.ds(a, n), my_rows, chunk(q)]
        d_c[q, g] = send(ref, ref, d_s.at[q, g], d_r.at[q, g], other_core)

    down_of = lambda j: 2 * j - 1 if j else 0
    up_of = lambda j: nz - 1 if j == half else 2 * j
    at = lambda p: pl.ds(p * rb, rb)
    ag_c = {}

    def ag_has(s, d, q):
        return s < half - 1 or q in SPLIT[d]

    def ag_send(s, d, q):
        of = (down_of, up_of)[d]
        ag_c[s, d, q] = send(
            rows.at[at(of(s)), chunk(q)],
            rows.at[at(of(s + 1)), chunk(q)],
            ag_s.at[d, s, q],
            ag_r.at[d, s, q],
            z_dev[d],
        )

    def scale_of(p, n):
        r = pl.ds(p * rb, n * rb)
        wide = rows[r, :].astype(f32)
        scales[r, :] = lax.rsqrt(jnp.mean(wide * wide, axis=-1, keepdims=True) + EPS)

    def ag_first(q):
        for dx in range(NX):
            if q or dx:
                tok[q, dx].wait_recv()
        for d in (0, 1):
            ag_send(0, d, q)

    def ag_step(s):
        for q in QORD:
            for d in (0, 1):
                if ag_has(s - 1, d, q):
                    ag_c[s - 1, d, q].wait_recv()
                if s < half and ag_has(s, d, q):
                    ag_send(s, d, q)
        if s == half:
            scale_of(nz - 1, 1)
        else:
            scale_of(down_of(s), 2)

    nt = (((1,), (1,)), ((), ()))

    def hidden(p, n):
        r = pl.ds(p * rb, n * rb)

        @pl.loop(0, 2)
        def _(c):
            f = pl.ds(pl.multiple_of(c * pair, pair), pair)
            s = scales[r, :]
            xr = rows[r, :]
            gate = s * lax.dot_general(xr, wbuf[0, f, :], nt, preferred_element_type=f32)
            up = s * lax.dot_general(xr, wbuf[1, f, :], nt, preferred_element_type=f32)
            hid[c, r, :] = (jax.nn.silu(gate) * up).astype(bf16)

    def project(p, n, q):
        r = pl.ds(p * rb, n * rb)
        part[r, chunk(q)] = jnp.dot(
            hid[0, r, :], wbuf[2, pl.ds(0, pair), chunk(q)], preferred_element_type=f32
        ) + jnp.dot(hid[1, r, :], wbuf[2, pl.ds(pair, pair), chunk(q)], preferred_element_type=f32)

    def gate_up_here():
        for q in QORD:
            d_c[q, 0].wait_recv()

    y_send(0)
    x_send(0, 0)
    y_send(1)
    rows[pl.ds(0, rb), lanes(tp)] = picked[prow(tp), :]
    for a in range(3):
        wbuf[a, my_rows, lanes(tp)] = wsrc[a, frow(y * NX + 2 * px, 2), :]

    def run(event):
        kind, rest = event[0], event[1:]
        if kind == "T":
            ag_first(int(rest))
        elif kind == "A":
            ag_step(int(rest))
        elif kind == "R":
            y_relay("ab".index(rest))
        elif kind == "H":
            gate_up_here()
            hidden(0, nz - 1)
        else:
            q, g = int(rest[0]), "ab".index(rest[1])
            {"X": x_send, "F": x_forward, "C": core_send}[kind](q, g)

    for event in ORDER:
        if event == "H":
            with scope("scale0"):
                scale_of(0, 1)
        with scope(event):
            run(event)

    with scope("hid_last"):
        hidden(nz - 1, 1)

    rs_c = {}

    def rs_step(s, q):
        for d in (0, 1):
            if s == 0 and q not in SPLIT[d]:
                continue
            p = (up_of, down_of)[d](half - s)
            acc = part[at(p), chunk(q)]
            if (s - 1, d, q) in rs_c:
                rs_c[s - 1, d, q].wait_recv()
                acc = acc + rs_in[d, s - 1, q].astype(f32)
            rs_out[d, s, q] = acc.astype(bf16)
            rs_c[s, d, q] = send(
                rs_out.at[d, s, q],
                rs_in.at[d, s, q],
                rs_s.at[d, s, q],
                rs_r.at[d, s, q],
                z_dev[d],
            )

    for q in QORD:
        with scope(f"rs0_{q}"):
            d_c[q, 1].wait_recv()
            project(nz - 1, 1, q)
            rs_step(0, q)
    with scope("project"):
        for q in QORD:
            project(0, nz - 1, q)
        outs = []
        for a, out in enumerate((gate_out, up_out, down_out)):
            c = pltpu.make_async_copy(wbuf.at[a, frow(2 * core + h, 1), :], out, out_s.at[a])
            c.start()
            outs.append(c)
    for s in range(1, half):
        with scope(f"rs{s}"):
            for q in QORD:
                rs_step(s, q)

    fin = []
    mine = prow(tp)
    for q in QORD:
        with scope(f"last{q}"):
            acc = part[at(0), chunk(q)]
            for d in (0, 1):
                rs_c[half - 1, d, q].wait_recv()
                acc = acc + rs_in[d, half - 1, q].astype(f32)
            eo[:, chunk(q)] = acc.astype(bf16)
            for dx in range(NX):
                if q or dx:
                    t = plane(NX - q, dx)
                    fin.append(
                        send(
                            eo.at[:, lanes(t)],
                            ret.at[mine, :],
                            fin_s.at[q, dx],
                            fin_r.at[q, dx],
                            {"tp": t},
                        )
                    )
    ret[mine, :] = eo[:, lanes(tp)]
    with scope("fin"):
        ids = lax.broadcasted_iota(jnp.int32, (tr, NT * rb), 1).astype(f32)
        hots = [jnp.where(ids == cols8[:, k : k + 1], 1.0, 0.0).astype(bf16) for k in (0, 1)]
        for c in fin:
            c.wait_recv()
    with scope("mix"):
        sent = [jnp.dot(m, ret[...], preferred_element_type=f32) for m in hots]
        mixed_out[...] = (cols8[:, 2:3] * sent[0] + cols8[:, 3:4] * sent[1]).astype(bf16)
    with scope("drain"):
        for c in outs:
            c.wait()
        for c in pending:
            c.wait_send()


def exchange(tokens, gain, gate, up, down, routes, logits, nz):
    tr = tokens.shape[0]
    width, fb = NT * LANES, gate.shape[0] // NT
    rb = 2 * tr // NT
    half = nz // 2
    bf16, f32 = jnp.bfloat16, jnp.float32
    dma = pltpu.SemaphoreType.DMA
    hbm = pl.BlockSpec(memory_space=pl.ANY)
    served = jax.ShapeDtypeStruct((fb, width), bf16)
    return pl.pallas_call(
        functools.partial(kernel, nz),
        name="exchange",
        out_shape=[served, served, served, jax.ShapeDtypeStruct((tr, LANES), bf16)],
        in_specs=[hbm] * 7,
        out_specs=[hbm, hbm, hbm, pl.BlockSpec(memory_space=pltpu.VMEM)],
        scratch_shapes=[
            pltpu.VMEM((tr, LANES), bf16),
            pltpu.VMEM((1, LANES), f32),
            pltpu.VMEM((3, NT * fb, LANES), f32),
            pltpu.VMEM((2, tr), jnp.int32),
            pltpu.VMEM((2, tr), f32),
            pltpu.VMEM((3, NT * fb, LANES), bf16),
            pltpu.VMEM((NT * rb, LANES), bf16),
            pltpu.VMEM((tr, 8), f32),
            pltpu.VMEM((nz * rb, width), bf16),
            pltpu.VMEM((nz * rb, 1), f32),
            pltpu.VMEM((NX - 1, 3, 2 * fb, LANES), bf16),
            pltpu.VMEM((2, 3, 2 * fb, LANES), bf16),
            pltpu.VMEM((3, 4 * fb, width), bf16),
            pltpu.VMEM((2, nz * rb, 2 * fb), bf16),
            pltpu.VMEM((nz * rb, width), f32),
            pltpu.VMEM((2, half, NX, rb, QC), bf16),
            pltpu.VMEM((2, half, NX, rb, QC), bf16),
            pltpu.VMEM((rb, width), bf16),
            pltpu.VMEM((NT * rb, LANES), bf16),
            dma((7,)),
            dma((NX, NX)),
            dma((NX, NX)),
            dma((2, half, NX)),
            dma((2, half, NX)),
            dma((NX - 1, NG, 2)),
            dma((NX - 1, NG, 2)),
            dma((NG, 2)),
            dma((NG, 2)),
            dma((NX, NG, 3)),
            dma((NX, NG, 3)),
            dma((NX, NG)),
            dma((NX, NG)),
            dma((2, half, NX)),
            dma((2, half, NX)),
            dma((NX, NX)),
            dma((NX, NX)),
            dma((3,)),
        ],
        compiler_params=pltpu.CompilerParams(collective_id=0, has_side_effects=True),
    )(tokens, gain, gate, up, down, routes, logits)


def local(tokens, norm_gain, gate_master, up_master, down_master, routes, route_logits):
    flat = lambda m: m.reshape(-1, LANES)
    nz = lax.axis_size("fs") // 2
    gate_serve, up_serve, down_serve, mixed = exchange(
        tokens,
        norm_gain[None, :],
        flat(gate_master),
        flat(up_master),
        flat(down_master),
        routes.T,
        route_logits.T,
        nz,
    )
    return (gate_serve[None], up_serve[None], down_serve[None], mixed)


def solution(mesh):
    weights = P(None, "fs", "tp")
    served = P("tp", "fs", None)
    return jax.shard_map(
        local,
        mesh=mesh,
        in_specs=(P("fs", "tp"), P("tp"), weights, weights, weights, P("fs"), P("fs")),
        out_specs=(served, served, served, P("fs", "tp")),
        check_vma=False,
    )
```

time: 115 us -> 94.8 us (0.82)
  the two profiles are of different devices: /device:TPU:8 before, /device:TPU:32 now
where the time goes in v2:
time: 94.8 us; the launch traced here: 94.6 us
  Pallas kernels  89.4 us (94%)
  local copies, waits for them, and re-layouts  4.55 us (5%)
    pallas_call x1, Pallas kernels, exchange(): pl.pallas_call(functools.partial(kernel, nz), name='exchange', out_shape=...  89.4 us
    unnamed x10, local copies, waits for them, and re-layouts  4.55 us

profile of v2, /device:TPU:32, one launch (start us, length us, event | category | flops | bytes accessed | tf_op | source)
XLA Modules:
  0.0 94.6 jit_solution(6589582209538702613)
XLA Ops:
  0.6 89.4 %exchange.1 = (bf16[112,2048]{1,0:T(8,128)(2,1)}, bf16[112,2048]{1,0:T(8,128)(2,1)}, bf16[112,2048]{1,0:T(8,128)(2,1)}, bf16[256,128]{1,0:T(8,128)(2,1)}) custom-call(bf16[256,128]{1,0:T(8,128)(2,1)} %tokens_h.1, f32[1,128]{1,0:T(1,128)} %bitcast.17, f32[1792,128]{1,0:T(8,128)} %bitcast.9, f32[1792,128]{1,0:T(8,128)} %bitcast.10, f32[1792,128]{1,0:T(8,128)} %bitcast.11, ...), custom_call_target="tpu_custom_call" | custom-call | tf_op jit(solution)/shard_map/exchange/pallas_call | solution.py:451
  90.0 0.0 copy-start.1
  90.0 1.9 %copy.15 = bf16[1,112,2048]{2,1,0:T(8,128)(2,1)} copy(bf16[1,112,2048]{2,1,0:T(8,128)(2,1)} %bitcast.14) | data formatting | bytes 917504
  91.9 0.0 copy-done.1
  91.9 0.0 copy-start
  91.9 0.8 copy.16
  92.7 0.4 copy-done
  93.1 0.0 copy-start.2
  93.1 0.8 copy.17
  93.8 0.1 copy-done.2
  93.9 0.6 copy.18
Async XLA Ops:
  90.0 1.9 %copy-start.1 = (bf16[112,2048]{1,0:T(8,128)(2,1)S(1)}, bf16[112,2048]{1,0:T(8,128)(2,1)}, u32[]{:S(2)}) copy-start(bf16[112,2048]{1,0:T(8,128)(2,1)} %get-tuple-element.9) | copy-start | bytes 1376260
  91.9 1.2 %copy-start = (bf16[112,2048]{1,0:T(8,128)(2,1)S(1)}, bf16[112,2048]{1,0:T(8,128)(2,1)}, u32[]{:S(2)}) copy-start(bf16[112,2048]{1,0:T(8,128)(2,1)} %get-tuple-element.10) | copy-start | bytes 1376260
  93.1 0.9 copy-start.2
